TPU v7x, 32 devices: a whole 2x2x4 slice. The times are simulated.
32 devices in a mesh: ep: 8 (over z, y), tp: 4 (over x, core).
Axes of the slice: x: 2, y: 2, z: 4, core: 2. Of those that a mesh axis runs over, the one named last changes fastest.
Arguments:
- att_queries: bfloat16 [8192, 1024], P(('ep', 'tp')), may hold values from -8 to 8
- att_keys: bfloat16 [8192, 256], P(('ep', 'tp')), may hold values from -6 to 6
- att_values: bfloat16 [8192, 256], P(('ep', 'tp')), may hold values from -6 to 6
- sink_logits: float32 [16], replicated, may hold values from 3 to 6.5
- out_weight: bfloat16 [1024, 2048], replicated, may hold values from -0.1875 to 0.1875
- att_gain: float32 [2048], replicated, may hold values from 0.1 to 1.9
- moe_in: bfloat16 [4096, 2048], P(('ep', 'tp')), may hold values from -6 to 6
- pre_gain: float32 [2048], replicated, may hold values from 0.1 to 1.9
- expert_ids: int32 [4096, 2], P(('ep', 'tp')), may hold values from 0 to 15, all different within a row; in each aligned block of 128 rows (0 to 127, 128 to 255, ...) at most 32 rows name the same one
- routed_expert_weight: float32 [4096, 2], P(('ep', 'tp')), may hold values from 0.2 to 1.5
- w_gate: bfloat16 [16, 2048, 768], P('ep', None, 'tp'), may hold values from -0.125 to 0.125
- w_up: bfloat16 [16, 2048, 768], P('ep', None, 'tp'), may hold values from -0.125 to 0.125
- w_down: bfloat16 [16, 768, 2048], P('ep', 'tp'), may hold values from -0.21875 to 0.21875
- common_expert_gate_weight: bfloat16 [2048, 512], P(None, 'tp'), may hold values from -0.125 to 0.125
- common_expert_up_weight: bfloat16 [2048, 512], P(None, 'tp'), may hold values from -0.125 to 0.125
- common_expert_down_weight: bfloat16 [512, 2048], P('tp'), may hold values from -0.25 to 0.25
- moe_gain: float32 [2048], replicated, may hold values from 0.1 to 1.9
Outputs:
- mixer_out: bfloat16 [8192, 2048], P(('ep', 'tp'))
- experts_out: bfloat16 [4096, 2048], P(('ep', 'tp'))
Inputs may be any that keep to these rules, and one draw needn't show every extreme that they name: `expert_ids`: each row names 2 different experts; within the rows of one device no expert is named more than 32 times, and in every draw some expert is named exactly 32 times by the rows of some device.
All inputs are finite; a program needn't handle non-finite values.
Results may differ from a plain program's by a relative error of at most 0.012.
Values may be sent and summed in bfloat16 or wider, within the bound.
A program may use at most 128 MiB of HBM per device.

v0:
```python
import functools
import math

import jax
import jax.numpy as jnp
from jax import lax
from jax.experimental import pallas as pl
from jax.experimental.pallas import tpu as pltpu
from jax.sharding import PartitionSpec as P

HEADS = 16
KV_HEADS = 4
HEAD_DIM = 64
WINDOW = 128

EPS = 1e-06
NEGATIVE = -1e30
PLANES = 2
CHUNKS = 4
ROW_TILE = 8

VMEM = pl.BlockSpec(memory_space=pltpu.VMEM)
SMEM = pl.BlockSpec(memory_space=pltpu.SMEM)
ANY = pl.BlockSpec(memory_space=pl.ANY)
F32 = jnp.float32
BF16 = jnp.bfloat16
MESH = pl.DeviceIdType.MESH
NT = (((1,), (1,)), ((), ()))
TN = (((0,), (0,)), ((), ()))


def iota(shape, dim):
    return lax.broadcasted_iota(jnp.int32, shape, dim)


def rms_scale(inputs, gain_vec):
    mean_sq = jnp.mean(inputs * inputs, axis=-1, keepdims=True)
    return inputs * lax.rsqrt(mean_sq + EPS) * gain_vec


def silu(v):
    return v / (1.0 + jnp.exp(-v))


def flip(index, amount):
    bit = 1
    while bit <= amount:
        if amount & bit:
            index = index + bit - 2 * bit * lax.rem(index // bit, 2)
        bit *= 2
    return index


class Sems:
    def __init__(self, *arrays):
        self.arrays, self.used = arrays, 0

    def take(self):
        self.used += 1
        return [array.at[self.used - 1] for array in self.arrays]


def layer_kernel(
    n_ep,
    n_tp,
    cap,
    sink_ref,
    ids_ref,
    weight_ref,
    pre_gain_ref,
    att_gain_ref,
    moe_gain_ref,
    q_hbm,
    k_hbm,
    v_hbm,
    out_w_hbm,
    x_hbm,
    gate_hbm,
    up_hbm,
    down_hbm,
    common_gate_hbm,
    common_up_hbm,
    common_down_hbm,
    mixer_hbm,
    experts_ref,
    x_v,
    normed,
    far_normed,
    far_ids,
    far_weight,
    chosen,
    packed,
    arrived,
    outs,
    returned,
    gate_v,
    up_v,
    down_v,
    act,
    hidden,
    common_gate,
    common_up,
    common_down,
    shared,
    part_out,
    part_in,
    q_v,
    k_v,
    v_v,
    rim_k,
    rim_v,
    out_w,
    mix,
    mixer,
    local_sems,
    send_sems,
    recv_sems,
    row_send,
    row_recv,
    ack_sem,
):
    far = n_tp // PLANES
    tokens, d = x_v.shape
    top = ids_ref.shape[0]
    slots = n_ep * cap
    width = gate_hbm.shape[1]
    half = far * width
    cw = d // CHUNKS
    me_e, me_t = lax.axis_index("ep"), lax.axis_index("tp")
    plane = me_t // far
    away = flip(me_t, far)
    mates = [flip(me_t, j) for j in range(1, far)]
    devices = n_ep * n_tp
    me = me_e * n_tp + me_t
    after, before = lax.rem(me + 1, devices), lax.rem(me + devices - 1, devices)
    local, net = Sems(local_sems), Sems(send_sems, recv_sems)
    sent = []

    def fetch(src, dst):
        copy = pltpu.make_async_copy(src, dst, local.take()[0])
        copy.start()
        return copy

    def remote(src, dst, e, t, start=True):
        send, recv = net.take()
        copy = pltpu.make_async_remote_copy(
            src, dst, send, recv, device_id=(e, t), device_id_type=MESH
        )
        if start:
            copy.start()
        sent.append(copy)
        return copy

    def rows_of(group):
        return pl.ds(pl.multiple_of(group * cap, cap), cap)

    def exchange(phase, src, dst, act_on):
        def step(j, carry):
            to = lax.rem(me_e + j, n_ep)
            copy = pltpu.make_async_remote_copy(
                src.at[rows_of(to)],
                dst.at[rows_of(me_e)],
                row_send.at[phase, j],
                row_recv.at[phase, j],
                device_id=(to, me_t),
                device_id_type=MESH,
            )
            act_on(copy)
            return carry

        lax.fori_loop(1, n_ep, step, 0)

    def start_rows(phase, src, dst):
        exchange(phase, src, dst, lambda copy: copy.start())
        dst[rows_of(me_e), :] = src[rows_of(me_e), :]

    def wait_rows(phase, src, dst):
        exchange(phase, src, dst, lambda copy: copy.wait_recv())

    load_x = fetch(x_hbm, x_v)
    barrier = pltpu.get_barrier_semaphore()

    def greet(j, carry):
        pl.semaphore_signal(
            barrier, inc=1, device_id=(lax.rem(me_e + j, n_ep), me_t), device_id_type=MESH
        )
        return carry

    lax.fori_loop(1, n_ep, greet, 0)
    for t in [away] + mates:
        pl.semaphore_signal(barrier, inc=1, device_id=(me_e, t), device_id_type=MESH)
    for n in (after, before):
        pl.semaphore_signal(
            barrier, inc=1, device_id=(n // n_tp, lax.rem(n, n_tp)), device_id_type=MESH
        )
    own_loads = []
    for src, dst in ((gate_hbm, gate_v), (up_hbm, up_v), (down_hbm, down_v)):
        own_loads.append(fetch(src.at[plane], dst.at[0]))
    load_q = [fetch(q_hbm, q_v), fetch(k_hbm, k_v), fetch(v_hbm, v_v), fetch(out_w_hbm, out_w)]
    common_cols = common_gate_hbm.shape[1]
    common_loads = [
        fetch(common_gate_hbm, common_gate.at[:, pl.ds(0, common_cols)]),
        fetch(common_up_hbm, common_up.at[:, pl.ds(0, common_cols)]),
        fetch(common_down_hbm, common_down.at[pl.ds(0, common_cols)]),
    ]
    pl.semaphore_wait(barrier, n_ep - 1 + far + 2)

    cut = width // 4
    first_rows, last_rows = pl.ds(0, cut), pl.ds(cut, width - cut)
    other = PLANES - 1 - plane
    gate_far = [
        remote(gate_hbm.at[other, first_rows], gate_v.at[far, first_rows], me_e, away),
    ]
    meta = [
        remote(ids_ref, far_ids, me_e, away),
        remote(weight_ref, far_weight, me_e, away),
    ]
    mate_common, mate_kept = [], []
    for j, t in enumerate(mates, 1):
        cols = pl.ds(j * common_cols, common_cols)
        mate_common.append(remote(common_gate_hbm, common_gate.at[:, cols], me_e, t))
        mate_common.append(remote(common_up_hbm, common_up.at[:, cols], me_e, t))
        mate_common.append(remote(common_down_hbm, common_down.at[cols], me_e, t))
    edge = k_hbm.shape[0] - WINDOW
    after_at = (after // n_tp, lax.rem(after, n_tp))
    rims = [
        remote(k_hbm.at[pl.ds(edge, WINDOW)], rim_k, *after_at),
        remote(v_hbm.at[pl.ds(edge, WINDOW)], rim_v, *after_at),
    ]

    load_x.wait()
    normed[...] = rms_scale(x_v[...].astype(F32), pre_gain_ref[...]).astype(BF16)
    normed_far = remote(normed, far_normed, me_e, away)
    gate_far.append(remote(gate_hbm.at[other, last_rows], gate_v.at[far, last_rows], me_e, away))
    up_halves = [pl.ds(0, width // 2), pl.ds(width // 2, width // 2)]
    up_far = [
        remote(up_hbm.at[other, rows], up_v.at[far, rows], me_e, away) for rows in up_halves
    ]
    chunks = [pl.ds(c * cw, cw) for c in range(CHUNKS)]
    down_far = [
        remote(down_hbm.at[other, :, cols], down_v.at[far, :, cols], me_e, away)
        for cols in chunks
    ]

    earlier = (iota((tokens, tokens), 0) < iota((tokens, tokens), 1)).astype(F32).astype(BF16)

    def route(ids, side):
        numbers = iota((n_ep, tokens), 0) * PLANES + plane
        hits = [numbers == ids[k : k + 1, :] for k in range(top)]
        hit = functools.reduce(lambda a, b: a | b, hits).astype(F32).astype(BF16)
        count = jnp.dot(hit, earlier, preferred_element_type=F32)
        place = count + (iota((n_ep, tokens), 0) * cap + 1).astype(F32)
        slot_number = (iota((slots, tokens), 0) + 1).astype(F32)
        total = None
        for k in range(top):
            slot = jnp.sum(jnp.where(hits[k], place, 0.0), axis=0, keepdims=True)
            one_hot = (slot_number == slot).astype(F32).astype(BF16)
            chosen[side, :, k * tokens : (k + 1) * tokens] = one_hot
            total = one_hot if total is None else total + one_hot
        return total

    def pack(ids, side, rows_ref):
        one_hot = route(ids, side)
        rows = rows_ref[...]
        step = slots // 2
        for i in range(2):
            packed[side, i * step : (i + 1) * step, :] = jnp.dot(
                one_hot[i * step : (i + 1) * step], rows, preferred_element_type=F32
            ).astype(BF16)
        start_rows(side, packed.at[side], arrived.at[side])

    pack(ids_ref[...], 0, normed)
    for j, t in enumerate(mates, 1):
        for src, dst in ((gate_hbm, gate_v), (up_hbm, up_v), (down_hbm, down_v)):
            mate_kept.append(remote(src.at[plane], dst.at[j], me_e, t))

    group_size = HEADS // KV_HEADS
    blocks = q_v.shape[0] // WINDOW
    shape = (WINDOW, 2 * WINDOW)
    gap = iota(shape, 0) + WINDOW - iota(shape, 1)
    inside = (gap >= 0) & (gap < WINDOW)

    def attend(n):
        rows = pl.ds(n * WINDOW, WINDOW)
        valid = inside
        if n == 0:
            valid = inside & (iota(shape, 1) + me * q_v.shape[0] >= WINDOW)
        for g in range(KV_HEADS):
            cols = pl.ds(g * HEAD_DIM, HEAD_DIM)
            if n == 0:
                keys = jnp.concatenate([rim_k[:, cols], k_v[rows, cols]], axis=0)
                values = jnp.concatenate([rim_v[:, cols], v_v[rows, cols]], axis=0)
            else:
                band = pl.ds((n - 1) * WINDOW, 2 * WINDOW)
                keys, values = k_v[band, cols], v_v[band, cols]
            mixed = []
            for j in range(group_size):
                h = g * group_size + j
                query = q_v[rows, pl.ds(h * HEAD_DIM, HEAD_DIM)]
                scores = lax.dot_general(query, keys, NT, preferred_element_type=F32) * (
                    1.0 / math.sqrt(HEAD_DIM)
                )
                scores = jnp.where(valid, scores, NEGATIVE)
                sink = sink_ref[h]
                row_top = jnp.maximum(jnp.max(scores, axis=-1, keepdims=True), sink)
                weights = jnp.exp(scores - row_top)
                total = jnp.sum(weights, axis=-1, keepdims=True) + jnp.exp(sink - row_top)
                probs = (weights * (1.0 / total)).astype(BF16)
                mixed.append(jnp.dot(probs, values, preferred_element_type=F32).astype(BF16))
            span = group_size * HEAD_DIM
            mix[rows, pl.ds(g * span, span)] = jnp.concatenate(mixed, axis=1)

    def project(n):
        rows = pl.ds(n * WINDOW, WINDOW)
        projected = jnp.dot(mix[rows, :], out_w[...], preferred_element_type=F32)
        mixer[rows, :] = rms_scale(projected, att_gain_ref[...]).astype(BF16)
        return fetch(mixer.at[rows], mixer_hbm.at[rows])

    def relay(copy, view):
        copy.wait_recv()
        return [remote(view(far), view(far + j), me_e, t) for j, t in enumerate(mates, 1)]

    for load in load_q[:3]:
        load.wait()
    for n in range(1, blocks):
        attend(n)
    gate_mate = relay(gate_far[0], lambda b: gate_v.at[b, first_rows])
    for copy in rims:
        copy.wait_recv()
    before_at = (before // n_tp, lax.rem(before, n_tp))
    pl.semaphore_signal(ack_sem, inc=1, device_id=before_at, device_id_type=MESH)
    attend(0)
    load_q[3].wait()
    mixer_copies = [project(n) for n in range(blocks)]

    def share(side, rows_ref):
        rows = rows_ref[...]
        gate = jnp.dot(rows, common_gate[...], preferred_element_type=F32)
        up = jnp.dot(rows, common_up[...], preferred_element_type=F32)
        units = (silu(gate) * up).astype(BF16)
        shared[side] = jnp.dot(units, common_down[...], preferred_element_type=F32)

    for load in common_loads:
        load.wait()
    for copy in mate_common:
        copy.wait_recv()
    share(0, normed)

    for copy in meta:
        copy.wait_recv()
    normed_far.wait_recv()
    pack(far_ids[...], 1, far_normed)
    share(1, far_normed)

    def product(side, weights, low, count):
        rows = arrived[side]
        matrix = weights[low : low + count].reshape(count * width, d)
        return lax.dot_general(rows, matrix, NT, preferred_element_type=F32)

    gate_mate += relay(gate_far[1], lambda b: gate_v.at[b, last_rows])
    for load in own_loads:
        load.wait()
    for copy in mate_kept:
        copy.wait_recv()
    for copy in gate_mate:
        copy.wait_recv()
    wait_rows(0, packed.at[0], arrived.at[0])
    act[0] = silu(product(0, gate_v, 0, 2 * far))
    hidden[0, :, :half] = (act[0, :, :half] * product(0, up_v, 0, far)).astype(BF16)
    up_mate = relay(up_far[0], lambda b: up_v.at[b, up_halves[0]])
    wait_rows(1, packed.at[1], arrived.at[1])
    act[1] = silu(product(1, gate_v, 0, 2 * far))
    hidden[1, :, :half] = (act[1, :, :half] * product(1, up_v, 0, far)).astype(BF16)
    up_mate += relay(up_far[1], lambda b: up_v.at[b, up_halves[1]])
    for copy in up_mate:
        copy.wait_recv()
    for side in range(2):
        hidden[side, :, half:] = (act[side, :, half:] * product(side, up_v, far, far)).astype(BF16)

    def phase(side, c):
        return 2 + side * CHUNKS + c

    down_mate = []
    for c, cols in enumerate(chunks):
        for copy in relay(down_far[c], lambda b, cols=cols: down_v.at[b, :, cols]):
            copy.wait_recv()
        matrix = down_v[:, :, cols].reshape(2 * half, cw)
        for side in (1, 0) if c else (0, 1):
            outs[side, c] = jnp.dot(hidden[side], matrix, preferred_element_type=F32).astype(BF16)
            start_rows(phase(side, c), outs.at[side, c], returned.at[side, c])

    eye = iota((tokens, tokens), 0) == iota((tokens, tokens), 1)

    def columns_of(weights):
        return [
            jnp.sum(jnp.where(eye, weights[k : k + 1, :], 0.0), axis=1, keepdims=True)
            for k in range(top)
        ]

    scales = [columns_of(weight_ref[...]), columns_of(far_weight[...])]

    def combine(side, c):
        wait_rows(phase(side, c), outs.at[side, c], returned.at[side, c])
        picked = lax.dot_general(
            chosen[side], returned[side, c], TN, preferred_element_type=F32
        )
        total = shared[side, :, chunks[c]]
        for k in range(top):
            total = total + scales[side][k] * picked[k * tokens : (k + 1) * tokens]
        return total

    parts = []
    for c, cols in enumerate(chunks):
        for side in (1, 0) if c else (0, 1):
            if side:
                part_out[c] = combine(1, c).astype(BF16)
                parts.append(remote(part_out.at[c], part_in.at[c], me_e, away))
            else:
                shared[0, :, cols] = combine(0, c)
    square = jnp.zeros((tokens, 1), F32)
    for c, cols in enumerate(chunks):
        parts[c].wait_recv()
        total = shared[0, :, cols] + part_in[c].astype(F32)
        shared[0, :, cols] = total
        square = square + jnp.sum(total * total, axis=-1, keepdims=True)
    scale = lax.rsqrt(square * (1.0 / d) + EPS)
    experts_ref[...] = (shared[0] * scale * moe_gain_ref[...]).astype(BF16)

    for copy in mixer_copies:
        copy.wait()
    for copy in sent:
        copy.wait_send()
    for side in range(2):
        exchange(side, packed.at[side], arrived.at[side], lambda copy: copy.wait_send())
        for c in range(CHUNKS):
            exchange(
                phase(side, c),
                outs.at[side, c],
                returned.at[side, c],
                lambda copy: copy.wait_send(),
            )
    pl.semaphore_wait(ack_sem, 1)


def body(
    att_queries,
    att_keys,
    att_values,
    sink_logits,
    out_weight,
    att_gain,
    moe_in,
    pre_gain,
    expert_ids,
    routed_expert_weight,
    w_gate,
    w_up,
    w_down,
    common_expert_gate_weight,
    common_expert_up_weight,
    common_expert_down_weight,
    moe_gain,
):
    assert w_gate.shape[0] == PLANES
    n_ep, n_tp = lax.axis_size("ep"), lax.axis_size("tp")
    rows, width = att_queries.shape
    tokens, d = moe_in.shape
    top = expert_ids.shape[1]
    slot_cap = 2 * tokens * top // (PLANES * n_ep)
    cap = -(-slot_cap // ROW_TILE) * ROW_TILE
    slots = cap * n_ep
    far = n_tp // PLANES
    blocks = 2 * far
    kv = att_keys.shape[1]
    units = w_gate.shape[2]
    common = common_expert_gate_weight.shape[1]
    cw = d // CHUNKS
    scratch = [
        pltpu.VMEM((tokens, d), BF16),
        pltpu.VMEM((tokens, d), BF16),
        pltpu.VMEM((tokens, d), BF16),
        pltpu.VMEM((top, tokens), jnp.int32),
        pltpu.VMEM((top, tokens), F32),
        pltpu.VMEM((2, slots, top * tokens), BF16),
        pltpu.VMEM((2, slots, d), BF16),
        pltpu.VMEM((2, slots, d), BF16),
        pltpu.VMEM((2, CHUNKS, slots, cw), BF16),
        pltpu.VMEM((2, CHUNKS, slots, cw), BF16),
        pltpu.VMEM((blocks, units, d), BF16),
        pltpu.VMEM((blocks, units, d), BF16),
        pltpu.VMEM((blocks, units, d), BF16),
        pltpu.VMEM((2, slots, blocks * units), F32),
        pltpu.VMEM((2, slots, blocks * units), BF16),
        pltpu.VMEM((d, far * common), BF16),
        pltpu.VMEM((d, far * common), BF16),
        pltpu.VMEM((far * common, d), BF16),
        pltpu.VMEM((2, tokens, d), F32),
        pltpu.VMEM((CHUNKS, tokens, cw), BF16),
        pltpu.VMEM((CHUNKS, tokens, cw), BF16),
        pltpu.VMEM((rows, width), BF16),
        pltpu.VMEM((rows, kv), BF16),
        pltpu.VMEM((rows, kv), BF16),
        pltpu.VMEM((WINDOW, kv), BF16),
        pltpu.VMEM((WINDOW, kv), BF16),
        pltpu.VMEM(out_weight.shape, BF16),
        pltpu.VMEM((rows, width), BF16),
        pltpu.VMEM((rows, d), BF16),
        pltpu.SemaphoreType.DMA((11 + rows // WINDOW,)),
        pltpu.SemaphoreType.DMA((9 + 2 * CHUNKS + (far - 1) * (10 + CHUNKS),)),
        pltpu.SemaphoreType.DMA((9 + 2 * CHUNKS + (far - 1) * (10 + CHUNKS),)),
        pltpu.SemaphoreType.DMA((2 + 2 * CHUNKS, n_ep)),
        pltpu.SemaphoreType.DMA((2 + 2 * CHUNKS, n_ep)),
        pltpu.SemaphoreType.REGULAR,
    ]
    return pl.pallas_call(
        functools.partial(layer_kernel, n_ep, n_tp, cap),
        out_shape=(
            jax.ShapeDtypeStruct((rows, d), BF16),
            jax.ShapeDtypeStruct((tokens, d), BF16),
        ),
        in_specs=[SMEM] + [VMEM] * 5 + [ANY] * 11,
        out_specs=(ANY, VMEM),
        scratch_shapes=scratch,
        compiler_params=pltpu.CompilerParams(
            vmem_limit_bytes=63 * 1024 * 1024, collective_id=0, has_side_effects=True
        ),
        name="layer",
    )(
        sink_logits,
        expert_ids.T,
        routed_expert_weight.T,
        pre_gain[None],
        att_gain[None],
        moe_gain[None],
        att_queries,
        att_keys,
        att_values,
        out_weight,
        moe_in,
        jnp.swapaxes(w_gate, 1, 2),
        jnp.swapaxes(w_up, 1, 2),
        w_down,
        common_expert_gate_weight,
        common_expert_up_weight,
        common_expert_down_weight,
    )


def solution(mesh):
    tokens_spec = P(("ep", "tp"), None)
    in_specs = (
        tokens_spec,
        tokens_spec,
        tokens_spec,
        P(),
        P(),
        P(),
        tokens_spec,
        P(),
        tokens_spec,
        tokens_spec,
        P("ep", None, "tp"),
        P("ep", None, "tp"),
        P("ep", "tp", None),
        P(None, "tp"),
        P(None, "tp"),
        P("tp", None),
        P(),
    )
    return jax.shard_map(
        body, mesh=mesh, in_specs=in_specs, out_specs=(tokens_spec, tokens_spec), check_vma=False
    )
```

profile of v0, /device:TPU:0, one launch (start us, length us, event | category | flops | bytes accessed | tf_op | source)
XLA Modules:
  0.0 115.8 jit_solution(2515033059519473860)
XLA Ops:
  0.6 111.9 %layer.1 = (bf16[256,2048]{1,0:T(8,128)(2,1)}, bf16[128,2048]{1,0:T(8,128)(2,1)}) custom-call(f32[16]{0:T(128)} %sink_ref.1, s32[2,128]{1,0:T(2,128)} %bitcast.12, f32[2,128]{1,0:T(2,128)} %bitcast.13, f32[1,2048]{1,0:T(1,128)} %bitcast.9, f32[1,2048]{1,0:T(1,128)} %bitcast.10, f32[1,2048]{1,0:T(1,128)} %bitcast.11, bf16[256,1024]{1,0:T(8,128)(2,1)} %q_hbm.1, ...), custom_call_target="tpu_custom_call" | custom-call | tf_op jit(solution)/shard_map/layer/pallas_call | solution.py:515
  112.6 0.0 copy-start
  112.6 2.4 %copy.21 = bf16[256,2048]{1,0:T(8,128)(2,1)} copy(bf16[256,2048]{1,0:T(8,128)(2,1)} %get-tuple-element.4) | data formatting | bytes 2097152
  115.0 0.0 copy-done
  115.0 0.8 copy.22
Async XLA Ops:
  112.6 2.4 %copy-start = (bf16[128,2048]{1,0:T(8,128)(2,1)S(1)}, bf16[128,2048]{1,0:T(8,128)(2,1)}, u32[]{:S(2)}) copy-start(bf16[128,2048]{1,0:T(8,128)(2,1)} %get-tuple-element.5) | copy-start | bytes 1572868
where the time goes:
time: 116 us
  Pallas kernels  112 us (97%)
  local copies, waits for them, and re-layouts  3.16 us (3%)
    pallas_call x1, Pallas kernels, body(): pl.pallas_call(functools.partial(layer_kernel, n_ep, n_tp, cap), out_shap...  112 us
    unnamed x4, local copies, waits for them, and re-layouts  3.16 us

commit v1 on v0

--- a/solution.py
+++ b/solution.py
@@ -17,7 +17,11 @@
 NEGATIVE = -1e30
 PLANES = 2
 CHUNKS = 4
+AHEAD = 2
+EARLY = 2
 ROW_TILE = 8
+PAIR = 2
+LINE = 4
 
 VMEM = pl.BlockSpec(memory_space=pltpu.VMEM)
 SMEM = pl.BlockSpec(memory_space=pltpu.SMEM)
@@ -81,7 +85,7 @@
     common_gate_hbm,
     common_up_hbm,
     common_down_hbm,
-    mixer_hbm,
+    mixer_ref,
     experts_ref,
     x_v,
     normed,
@@ -111,17 +115,32 @@
     rim_v,
     out_w,
     mix,
-    mixer,
     local_sems,
     send_sems,
     recv_sems,
     row_send,
     row_recv,
     ack_sem,
+    *merge_refs,
 ):
     far = n_tp // PLANES
     tokens, d = x_v.shape
     top = ids_ref.shape[0]
+    merging = bool(merge_refs)
+    if merging:
+        (
+            home_ids,
+            home_weight,
+            home_chosen,
+            home_rows,
+            home_sums,
+            home_out,
+            home_in,
+            meta_send,
+            meta_recv,
+            home_send,
+            home_recv,
+        ) = merge_refs
     slots = n_ep * cap
     width = gate_hbm.shape[1]
     half = far * width
@@ -134,6 +153,14 @@
     me = me_e * n_tp + me_t
     after, before = lax.rem(me + 1, devices), lax.rem(me + devices - 1, devices)
     local, net = Sems(local_sems), Sems(send_sems, recv_sems)
+
+    line, spot = me_e // PAIR, lax.rem(me_e, PAIR)
+    last = LINE - 1
+    upper = line // (LINE // 2)
+    home_line = last * (1 - upper)
+    at_end = lax.rem(line, last) == 0
+    end_flag = 1 - (lax.rem(line, last) + 1) // 2
+    pair_e = line * PAIR + 1 - spot
     sent = []
 
     def fetch(src, dst):
@@ -154,8 +181,9 @@
     def rows_of(group):
         return pl.ds(pl.multiple_of(group * cap, cap), cap)
 
-    def exchange(phase, src, dst, act_on):
-        def step(j, carry):
+    def exchange(phase, src, dst, act_on, wanted=None, first=1, stride=1):
+        def step(i, carry):
+            j = first + stride * i
             to = lax.rem(me_e + j, n_ep)
             copy = pltpu.make_async_remote_copy(
                 src.at[rows_of(to)],
@@ -165,17 +193,27 @@
                 device_id=(to, me_t),
                 device_id_type=MESH,
             )
-            act_on(copy)
+            if wanted is None:
+                act_on(copy)
+            else:
+                pl.when(wanted(j))(lambda: act_on(copy))
             return carry
 
-        lax.fori_loop(1, n_ep, step, 0)
-
-    def start_rows(phase, src, dst):
-        exchange(phase, src, dst, lambda copy: copy.start())
+        lax.fori_loop(0, (n_ep - first + stride - 1) // stride, step, 0)
+
+    def is_sent(j):
+        return lax.rem(me_e + j, n_ep) // PAIR != home_line
+
+    def is_received(j):
+        source = lax.rem(me_e + n_ep - j, n_ep) // PAIR
+        return line != last * (1 - source // (LINE // 2))
+
+    def keep_rows(src, dst):
         dst[rows_of(me_e), :] = src[rows_of(me_e), :]
 
-    def wait_rows(phase, src, dst):
-        exchange(phase, src, dst, lambda copy: copy.wait_recv())
+    def wait_rows(phase, src, dst, back=False):
+        wanted = is_received if back and merging else None
+        exchange(phase, src, dst, lambda copy: copy.wait_recv(), wanted)
 
     load_x = fetch(x_hbm, x_v)
     barrier = pltpu.get_barrier_semaphore()
@@ -193,6 +231,8 @@
         pl.semaphore_signal(
             barrier, inc=1, device_id=(n // n_tp, lax.rem(n, n_tp)), device_id_type=MESH
         )
+    if merging:
+        pl.semaphore_signal(barrier, inc=1, device_id=(pair_e, away), device_id_type=MESH)
     own_loads = []
     for src, dst in ((gate_hbm, gate_v), (up_hbm, up_v), (down_hbm, down_v)):
         own_loads.append(fetch(src.at[plane], dst.at[0]))
@@ -203,7 +243,7 @@
         fetch(common_up_hbm, common_up.at[:, pl.ds(0, common_cols)]),
         fetch(common_down_hbm, common_down.at[pl.ds(0, common_cols)]),
     ]
-    pl.semaphore_wait(barrier, n_ep - 1 + far + 2)
+    pl.semaphore_wait(barrier, n_ep - 1 + far + 2 + int(merging))
 
     cut = width // 4
     first_rows, last_rows = pl.ds(0, cut), pl.ds(cut, width - cut)
@@ -228,6 +268,29 @@
         remote(v_hbm.at[pl.ds(edge, WINDOW)], rim_v, *after_at),
     ]
 
+    def home_meta(n):
+        lines = (LINE // 2 - upper, last - line)
+        to = lines[n] * PAIR + spot
+        return [
+            pltpu.make_async_remote_copy(
+                src,
+                dst,
+                meta_send.at[n, i],
+                meta_recv.at[i],
+                device_id=(to, me_t),
+                device_id_type=MESH,
+            )
+            for i, (src, dst) in enumerate(((ids_ref, home_ids), (weight_ref, home_weight)))
+        ]
+
+    if merging:
+
+        @pl.when(at_end)
+        def _():
+            for n in range(2):
+                for copy in home_meta(n):
+                    copy.start()
+
     load_x.wait()
     normed[...] = rms_scale(x_v[...].astype(F32), pre_gain_ref[...]).astype(BF16)
     normed_far = remote(normed, far_normed, me_e, away)
@@ -238,36 +301,37 @@
     ]
     chunks = [pl.ds(c * cw, cw) for c in range(CHUNKS)]
     down_far = [
-        remote(down_hbm.at[other, :, cols], down_v.at[far, :, cols], me_e, away)
-        for cols in chunks
+        remote(down_hbm.at[other, :, cols], down_v.at[far, :, cols], me_e, away, c < AHEAD)
+        for c, cols in enumerate(chunks)
     ]
 
     earlier = (iota((tokens, tokens), 0) < iota((tokens, tokens), 1)).astype(F32).astype(BF16)
 
-    def route(ids, side):
-        numbers = iota((n_ep, tokens), 0) * PLANES + plane
+    def route(ids, numbers, chosen_ref):
         hits = [numbers == ids[k : k + 1, :] for k in range(top)]
         hit = functools.reduce(lambda a, b: a | b, hits).astype(F32).astype(BF16)
         count = jnp.dot(hit, earlier, preferred_element_type=F32)
-        place = count + (iota((n_ep, tokens), 0) * cap + 1).astype(F32)
-        slot_number = (iota((slots, tokens), 0) + 1).astype(F32)
+        place = count + (iota(numbers.shape, 0) * cap + 1).astype(F32)
+        slot_number = (iota((chosen_ref.shape[0], tokens), 0) + 1).astype(F32)
         total = None
         for k in range(top):
             slot = jnp.sum(jnp.where(hits[k], place, 0.0), axis=0, keepdims=True)
             one_hot = (slot_number == slot).astype(F32).astype(BF16)
-            chosen[side, :, k * tokens : (k + 1) * tokens] = one_hot
+            chosen_ref[:, k * tokens : (k + 1) * tokens] = one_hot
             total = one_hot if total is None else total + one_hot
         return total
 
     def pack(ids, side, rows_ref):
-        one_hot = route(ids, side)
+        numbers = iota((n_ep, tokens), 0) * PLANES + plane
+        one_hot = route(ids, numbers, chosen.at[side])
         rows = rows_ref[...]
         step = slots // 2
         for i in range(2):
             packed[side, i * step : (i + 1) * step, :] = jnp.dot(
                 one_hot[i * step : (i + 1) * step], rows, preferred_element_type=F32
             ).astype(BF16)
-        start_rows(side, packed.at[side], arrived.at[side])
+        exchange(side, packed.at[side], arrived.at[side], lambda copy: copy.start())
+        keep_rows(packed.at[side], arrived.at[side])
 
     pack(ids_ref[...], 0, normed)
     for j, t in enumerate(mates, 1):
@@ -313,8 +377,7 @@
     def project(n):
         rows = pl.ds(n * WINDOW, WINDOW)
         projected = jnp.dot(mix[rows, :], out_w[...], preferred_element_type=F32)
-        mixer[rows, :] = rms_scale(projected, att_gain_ref[...]).astype(BF16)
-        return fetch(mixer.at[rows], mixer_hbm.at[rows])
+        mixer_ref[rows, :] = rms_scale(projected, att_gain_ref[...]).astype(BF16)
 
     def relay(copy, view):
         copy.wait_recv()
@@ -331,7 +394,8 @@
     pl.semaphore_signal(ack_sem, inc=1, device_id=before_at, device_id_type=MESH)
     attend(0)
     load_q[3].wait()
-    mixer_copies = [project(n) for n in range(blocks)]
+    for n in range(blocks):
+        project(n)
 
     def share(side, rows_ref):
         rows = rows_ref[...]
@@ -351,6 +415,23 @@
     normed_far.wait_recv()
     pack(far_ids[...], 1, far_normed)
     share(1, far_normed)
+
+    if merging:
+        block = iota((2 * PAIR, tokens), 0)
+        over_y, over_x = block // 2, lax.rem(block, 2)
+        group = line * PAIR + spot + over_y - 2 * spot * over_y
+        for copy in home_meta(0):
+            copy.wait_recv()
+        route(
+            home_ids[...], group * PLANES + plane + over_x - 2 * plane * over_x, home_chosen
+        )
+
+        @pl.when(at_end)
+        def _():
+            empty = pl.ds(pl.multiple_of((1 - upper) * (slots // 2), slots // 2), slots // 2)
+            for side in range(2):
+                for c in range(CHUNKS):
+                    returned[side, c, empty, :] = jnp.zeros((slots // 2, cw), BF16)
 
     def product(side, weights, low, count):
         rows = arrived[side]
@@ -380,15 +461,6 @@
     def phase(side, c):
         return 2 + side * CHUNKS + c
 
-    down_mate = []
-    for c, cols in enumerate(chunks):
-        for copy in relay(down_far[c], lambda b, cols=cols: down_v.at[b, :, cols]):
-            copy.wait_recv()
-        matrix = down_v[:, :, cols].reshape(2 * half, cw)
-        for side in (1, 0) if c else (0, 1):
-            outs[side, c] = jnp.dot(hidden[side], matrix, preferred_element_type=F32).astype(BF16)
-            start_rows(phase(side, c), outs.at[side, c], returned.at[side, c])
-
     eye = iota((tokens, tokens), 0) == iota((tokens, tokens), 1)
 
     def columns_of(weights):
@@ -397,26 +469,132 @@
             for k in range(top)
         ]
 
+    def weigh(total, columns, one_hot, rows):
+        picked = lax.dot_general(one_hot, rows, TN, preferred_element_type=F32)
+        for k in range(top):
+            part = columns[k] * picked[k * tokens : (k + 1) * tokens]
+            total = part if total is None else total + part
+        return total
+
+    def home_blocks(c):
+        routes = (
+            (1, home_line * PAIR + spot, me_e, away),
+            (0, home_line * PAIR + 1 - spot, pair_e, me_t),
+            (1, home_line * PAIR + 1 - spot, pair_e, away),
+        )
+        return [
+            pltpu.make_async_remote_copy(
+                outs.at[side, c, rows_of(home)],
+                home_rows.at[c, pl.ds(n * cap, cap)],
+                home_send.at[c, n],
+                home_recv.at[c, n],
+                device_id=(e, t),
+                device_id_type=MESH,
+            )
+            for n, (side, home, e, t) in enumerate(routes, 1)
+        ]
+
+    def home_step(c):
+        to = end_flag * (1 + line // last) + (1 - end_flag) * home_line
+        return pltpu.make_async_remote_copy(
+            home_out.at[c],
+            home_in.at[c],
+            home_send.at[c, 0],
+            home_recv.at[c, 0],
+            device_id=(to * PAIR + spot, me_t),
+            device_id_type=MESH,
+        )
+
+    def gather_home(c):
+        for copy in home_blocks(c):
+            copy.start()
+        home_rows[c, 0:cap, :] = outs[0, c, rows_of(home_line * PAIR + spot), :]
+
+    def sum_home(c):
+        for copy in home_blocks(c):
+            copy.wait_recv()
+        sums = weigh(None, home_columns, home_chosen[...], home_rows[c])
+
+        @pl.when(at_end)
+        def _():
+            home_out[c] = sums.astype(BF16)
+            home_step(c).start()
+
+        @pl.when(jnp.logical_not(at_end))
+        def _():
+            home_sums[c] = sums
+
+    def pass_home(c):
+        @pl.when(jnp.logical_not(at_end))
+        def _():
+            home_step(c).wait_recv()
+            home_out[c] = (home_sums[c] + home_in[c].astype(F32)).astype(BF16)
+            home_step(c).start()
+
+    if merging:
+        home_columns = columns_of(home_weight[...])
+
+    def send_back(side, c, first):
+        exchange(
+            phase(side, c),
+            outs.at[side, c],
+            returned.at[side, c],
+            lambda copy: copy.start(),
+            is_sent if merging else None,
+            first,
+            2,
+        )
+
+    for c, cols in enumerate(chunks):
+        for copy in relay(down_far[c], lambda b, cols=cols: down_v.at[b, :, cols]):
+            copy.wait_recv()
+        matrix = down_v[:, :, cols].reshape(2 * half, cw)
+        for side in range(2):
+            outs[side, c] = jnp.dot(hidden[side], matrix, preferred_element_type=F32).astype(BF16)
+        if merging:
+            gather_home(c)
+        if c + AHEAD < CHUNKS:
+            down_far[c + AHEAD].start()
+        if merging:
+            if c:
+                sum_home(c - 1)
+            if c == CHUNKS - 1:
+                sum_home(c)
+        for side in (1, 0):
+            send_back(side, c, 2)
+            if c < EARLY:
+                send_back(side, c, 1)
+            keep_rows(outs.at[side, c], returned.at[side, c])
+        if merging and c >= 2:
+            pass_home(c - 2)
+    for c in range(EARLY, CHUNKS):
+        for side in (1, 0):
+            send_back(side, c, 1)
+
     scales = [columns_of(weight_ref[...]), columns_of(far_weight[...])]
 
     def combine(side, c):
-        wait_rows(phase(side, c), outs.at[side, c], returned.at[side, c])
-        picked = lax.dot_general(
-            chosen[side], returned[side, c], TN, preferred_element_type=F32
-        )
-        total = shared[side, :, chunks[c]]
-        for k in range(top):
-            total = total + scales[side][k] * picked[k * tokens : (k + 1) * tokens]
-        return total
+        wait_rows(phase(side, c), outs.at[side, c], returned.at[side, c], True)
+        return weigh(shared[side, :, chunks[c]], scales[side], chosen[side], returned[side, c])
 
     parts = []
     for c, cols in enumerate(chunks):
-        for side in (1, 0) if c else (0, 1):
+        if merging and c % 2 == 0:
+            pass_home(CHUNKS - 2 + c // 2)
+        for side in (1, 0):
             if side:
                 part_out[c] = combine(1, c).astype(BF16)
                 parts.append(remote(part_out.at[c], part_in.at[c], me_e, away))
             else:
                 shared[0, :, cols] = combine(0, c)
+    if merging:
+
+        @pl.when(at_end)
+        def _():
+            for c, cols in enumerate(chunks):
+                home_step(c).wait_recv()
+                shared[0, :, cols] += home_in[c].astype(F32)
+
     square = jnp.zeros((tokens, 1), F32)
     for c, cols in enumerate(chunks):
         parts[c].wait_recv()
@@ -426,8 +604,6 @@
     scale = lax.rsqrt(square * (1.0 / d) + EPS)
     experts_ref[...] = (shared[0] * scale * moe_gain_ref[...]).astype(BF16)
 
-    for copy in mixer_copies:
-        copy.wait()
     for copy in sent:
         copy.wait_send()
     for side in range(2):
@@ -438,7 +614,19 @@
                 outs.at[side, c],
                 returned.at[side, c],
                 lambda copy: copy.wait_send(),
+                is_sent if merging else None,
             )
+    if merging:
+        for c in range(CHUNKS):
+            for copy in home_blocks(c) + [home_step(c)]:
+                copy.wait_send()
+
+        @pl.when(at_end)
+        def _():
+            for n in range(2):
+                for copy in home_meta(n):
+                    copy.wait_send()
+
     pl.semaphore_wait(ack_sem, 1)
 
 
@@ -504,25 +692,38 @@
         pltpu.VMEM((WINDOW, kv), BF16),
         pltpu.VMEM(out_weight.shape, BF16),
         pltpu.VMEM((rows, width), BF16),
-        pltpu.VMEM((rows, d), BF16),
-        pltpu.SemaphoreType.DMA((11 + rows // WINDOW,)),
+        pltpu.SemaphoreType.DMA((11,)),
         pltpu.SemaphoreType.DMA((9 + 2 * CHUNKS + (far - 1) * (10 + CHUNKS),)),
         pltpu.SemaphoreType.DMA((9 + 2 * CHUNKS + (far - 1) * (10 + CHUNKS),)),
         pltpu.SemaphoreType.DMA((2 + 2 * CHUNKS, n_ep)),
         pltpu.SemaphoreType.DMA((2 + 2 * CHUNKS, n_ep)),
         pltpu.SemaphoreType.REGULAR,
     ]
+    if n_ep == PAIR * LINE and far == 2:
+        scratch += [
+            pltpu.VMEM((top, tokens), jnp.int32),
+            pltpu.VMEM((top, tokens), F32),
+            pltpu.VMEM((2 * PAIR * cap, top * tokens), BF16),
+            pltpu.VMEM((CHUNKS, 2 * PAIR * cap, cw), BF16),
+            pltpu.VMEM((CHUNKS, tokens, cw), F32),
+            pltpu.VMEM((CHUNKS, tokens, cw), BF16),
+            pltpu.VMEM((CHUNKS, tokens, cw), BF16),
+            pltpu.SemaphoreType.DMA((2, 2)),
+            pltpu.SemaphoreType.DMA((2,)),
+            pltpu.SemaphoreType.DMA((CHUNKS, 4)),
+            pltpu.SemaphoreType.DMA((CHUNKS, 4)),
+        ]
     return pl.pallas_call(
         functools.partial(layer_kernel, n_ep, n_tp, cap),
         out_shape=(
-            jax.ShapeDtypeStruct((rows, d), BF16),
-            jax.ShapeDtypeStruct((tokens, d), BF16),
+            pltpu.VMEM((rows, d), BF16),
+            pltpu.VMEM((tokens, d), BF16),
         ),
         in_specs=[SMEM] + [VMEM] * 5 + [ANY] * 11,
-        out_specs=(ANY, VMEM),
+        out_specs=(VMEM, VMEM),
         scratch_shapes=scratch,
         compiler_params=pltpu.CompilerParams(
-            vmem_limit_bytes=63 * 1024 * 1024, collective_id=0, has_side_effects=True
+            vmem_limit_bytes=62 * 1024 * 1024 + 256 * 1024, collective_id=0, has_side_effects=True
         ),
         name="layer",
     )(

time: 116 us -> 106 us (0.914)
  Pallas kernels: 112 us -> 104 us
  local copies, waits for them, and re-layouts: 3.16 us -> 1.77 us
    pallas_call x1, Pallas kernels: 112 us -> 104 us  [body(): pl.pallas_call(functools.partial(layer_kernel, n_ep, n_tp, cap), out_shap...]
    unnamed x4 -> x2, local copies, waits for them, and re-layouts: 3.16 us -> 1.77 us
where the time goes in v1:
time: 106 us
  Pallas kernels  104 us (98%)
  local copies, waits for them, and re-layouts  1.77 us (2%)
    pallas_call x1, Pallas kernels, body(): pl.pallas_call(functools.partial(layer_kernel, n_ep, n_tp, cap), out_shap...  104 us

profile of v1, /device:TPU:0, one launch (start us, length us, event | category | flops | bytes accessed | tf_op | source)
XLA Modules:
  0.0 106.0 jit_solution(2752294911502573943)
XLA Ops:
  0.6 103.6 %layer.1 = (bf16[256,2048]{1,0:T(8,128)(2,1)S(1)}, bf16[128,2048]{1,0:T(8,128)(2,1)S(1)}) custom-call(f32[16]{0:T(128)} %sink_ref.1, s32[2,128]{1,0:T(2,128)} %bitcast.12, f32[2,128]{1,0:T(2,128)} %bitcast.13, f32[1,2048]{1,0:T(1,128)} %bitcast.9, f32[1,2048]{1,0:T(1,128)} %bitcast.10, f32[1,2048]{1,0:T(1,128)} %bitcast.11, bf16[256,1024]{1,0:T(8,128)(2,1)} %q_hbm.1, ...), custom_call_target="tpu_custom_call" | custom-call | tf_op jit(solution)/shard_map/layer/pallas_call | solution.py:716
  104.2 1.0 copy.21
  105.2 0.8 copy.22

commit v2 on v1

--- a/solution.py
+++ b/solution.py
@@ -16,7 +16,8 @@
 EPS = 1e-06
 NEGATIVE = -1e30
 PLANES = 2
-CHUNKS = 4
+WIDTHS = (2, 4, 4, 4, 2)
+CHUNKS = len(WIDTHS)
 AHEAD = 2
 EARLY = 2
 ROW_TILE = 8
@@ -144,7 +145,7 @@
     slots = n_ep * cap
     width = gate_hbm.shape[1]
     half = far * width
-    cw = d // CHUNKS
+    unit = d // sum(WIDTHS)
     me_e, me_t = lax.axis_index("ep"), lax.axis_index("tp")
     plane = me_t // far
     away = flip(me_t, far)
@@ -152,7 +153,7 @@
     devices = n_ep * n_tp
     me = me_e * n_tp + me_t
     after, before = lax.rem(me + 1, devices), lax.rem(me + devices - 1, devices)
-    local, net = Sems(local_sems), Sems(send_sems, recv_sems)
+    local, net, shared_sends = Sems(local_sems), Sems(recv_sems), Sems(send_sems)
 
     line, spot = me_e // PAIR, lax.rem(me_e, PAIR)
     last = LINE - 1
@@ -161,59 +162,83 @@
     at_end = lax.rem(line, last) == 0
     end_flag = 1 - (lax.rem(line, last) + 1) // 2
     pair_e = line * PAIR + 1 - spot
-    sent = []
+    sent = {}
 
     def fetch(src, dst):
         copy = pltpu.make_async_copy(src, dst, local.take()[0])
         copy.start()
         return copy
 
-    def remote(src, dst, e, t, start=True):
-        send, recv = net.take()
+    def remote(src, dst, e, t, name, start=True):
+        if name not in sent:
+            sent[name] = shared_sends.take()[0]
         copy = pltpu.make_async_remote_copy(
-            src, dst, send, recv, device_id=(e, t), device_id_type=MESH
+            src, dst, sent[name], net.take()[0], device_id=(e, t), device_id_type=MESH
         )
         if start:
             copy.start()
-        sent.append(copy)
         return copy
+
+    def settle(name, ref):
+        pltpu.make_async_remote_copy(
+            ref, ref, sent.pop(name), recv_sems.at[0], device_id=(me_e, away), device_id_type=MESH
+        ).wait_send()
 
     def rows_of(group):
         return pl.ds(pl.multiple_of(group * cap, cap), cap)
 
-    def exchange(phase, src, dst, act_on, wanted=None, first=1, stride=1):
+    def exchange(phase, src, dst, cols, wanted=None, first=1, stride=1):
         def step(i, carry):
             j = first + stride * i
             to = lax.rem(me_e + j, n_ep)
             copy = pltpu.make_async_remote_copy(
-                src.at[rows_of(to)],
-                dst.at[rows_of(me_e)],
-                row_send.at[phase, j],
-                row_recv.at[phase, j],
+                src.at[rows_of(to), cols],
+                dst.at[rows_of(me_e), cols],
+                row_send.at[min(phase, 2) // 2],
+                row_recv.at[phase],
                 device_id=(to, me_t),
                 device_id_type=MESH,
             )
             if wanted is None:
-                act_on(copy)
+                copy.start()
             else:
-                pl.when(wanted(j))(lambda: act_on(copy))
+                pl.when(wanted(j))(lambda: copy.start())
             return carry
 
         lax.fori_loop(0, (n_ep - first + stride - 1) // stride, step, 0)
+
+    def wait_rows(phase, dst, cols, peers):
+        view = dst.at[pl.ds(0, peers * cap), cols]
+        pltpu.make_async_remote_copy(
+            view,
+            view,
+            row_send.at[0],
+            row_recv.at[phase],
+            device_id=(me_e, away),
+            device_id_type=MESH,
+        ).wait_recv()
+
+    def wait_sent(kind, src, peers):
+        view = src.at[:, pl.ds(0, peers * cap)]
+        pltpu.make_async_remote_copy(
+            view,
+            view,
+            row_send.at[kind],
+            row_recv.at[0],
+            device_id=(me_e, away),
+            device_id_type=MESH,
+        ).wait_send()
 
     def is_sent(j):
         return lax.rem(me_e + j, n_ep) // PAIR != home_line
 
-    def is_received(j):
-        source = lax.rem(me_e + n_ep - j, n_ep) // PAIR
-        return line != last * (1 - source // (LINE // 2))
-
-    def keep_rows(src, dst):
-        dst[rows_of(me_e), :] = src[rows_of(me_e), :]
-
-    def wait_rows(phase, src, dst, back=False):
-        wanted = is_received if back and merging else None
-        exchange(phase, src, dst, lambda copy: copy.wait_recv(), wanted)
+    def keep_rows(src, dst, cols):
+        dst[rows_of(me_e), cols] = src[rows_of(me_e), cols]
+
+    everything = pl.ds(0, d)
+
+    def wait_dispatch(side):
+        wait_rows(side, arrived.at[side], everything, n_ep - 1)
 
     load_x = fetch(x_hbm, x_v)
     barrier = pltpu.get_barrier_semaphore()
@@ -249,23 +274,28 @@
     first_rows, last_rows = pl.ds(0, cut), pl.ds(cut, width - cut)
     other = PLANES - 1 - plane
     gate_far = [
-        remote(gate_hbm.at[other, first_rows], gate_v.at[far, first_rows], me_e, away),
+        remote(gate_hbm.at[other, first_rows], gate_v.at[far, first_rows], me_e, away, "gate"),
     ]
     meta = [
-        remote(ids_ref, far_ids, me_e, away),
-        remote(weight_ref, far_weight, me_e, away),
+        remote(ids_ref, far_ids, me_e, away, "ids"),
+        remote(weight_ref, far_weight, me_e, away, "weight"),
     ]
     mate_common, mate_kept = [], []
     for j, t in enumerate(mates, 1):
         cols = pl.ds(j * common_cols, common_cols)
-        mate_common.append(remote(common_gate_hbm, common_gate.at[:, cols], me_e, t))
-        mate_common.append(remote(common_up_hbm, common_up.at[:, cols], me_e, t))
-        mate_common.append(remote(common_down_hbm, common_down.at[cols], me_e, t))
+        for kind, (src, dst) in enumerate(
+            (
+                (common_gate_hbm, common_gate.at[:, cols]),
+                (common_up_hbm, common_up.at[:, cols]),
+                (common_down_hbm, common_down.at[cols]),
+            )
+        ):
+            mate_common.append(remote(src, dst, me_e, t, ("common", kind, j)))
     edge = k_hbm.shape[0] - WINDOW
     after_at = (after // n_tp, lax.rem(after, n_tp))
     rims = [
-        remote(k_hbm.at[pl.ds(edge, WINDOW)], rim_k, *after_at),
-        remote(v_hbm.at[pl.ds(edge, WINDOW)], rim_v, *after_at),
+        remote(k_hbm.at[pl.ds(edge, WINDOW)], rim_k, *after_at, "rim_k", False),
+        remote(v_hbm.at[pl.ds(edge, WINDOW)], rim_v, *after_at, "rim_v", False),
     ]
 
     def home_meta(n):
@@ -293,15 +323,19 @@
 
     load_x.wait()
     normed[...] = rms_scale(x_v[...].astype(F32), pre_gain_ref[...]).astype(BF16)
-    normed_far = remote(normed, far_normed, me_e, away)
-    gate_far.append(remote(gate_hbm.at[other, last_rows], gate_v.at[far, last_rows], me_e, away))
+    normed_far = remote(normed, far_normed, me_e, away, "normed")
+    gate_far.append(
+        remote(gate_hbm.at[other, last_rows], gate_v.at[far, last_rows], me_e, away, "gate")
+    )
     up_halves = [pl.ds(0, width // 2), pl.ds(width // 2, width // 2)]
     up_far = [
-        remote(up_hbm.at[other, rows], up_v.at[far, rows], me_e, away) for rows in up_halves
+        remote(up_hbm.at[other, rows], up_v.at[far, rows], me_e, away, "up") for rows in up_halves
     ]
-    chunks = [pl.ds(c * cw, cw) for c in range(CHUNKS)]
+    chunks = [pl.ds(sum(WIDTHS[:c]) * unit, WIDTHS[c] * unit) for c in range(CHUNKS)]
     down_far = [
-        remote(down_hbm.at[other, :, cols], down_v.at[far, :, cols], me_e, away, c < AHEAD)
+        remote(
+            down_hbm.at[other, :, cols], down_v.at[far, :, cols], me_e, away, "down", c < AHEAD
+        )
         for c, cols in enumerate(chunks)
     ]
 
@@ -330,13 +364,15 @@
             packed[side, i * step : (i + 1) * step, :] = jnp.dot(
                 one_hot[i * step : (i + 1) * step], rows, preferred_element_type=F32
             ).astype(BF16)
-        exchange(side, packed.at[side], arrived.at[side], lambda copy: copy.start())
-        keep_rows(packed.at[side], arrived.at[side])
+        exchange(side, packed.at[side], arrived.at[side], everything)
+        keep_rows(packed.at[side], arrived.at[side], everything)
 
     pack(ids_ref[...], 0, normed)
     for j, t in enumerate(mates, 1):
-        for src, dst in ((gate_hbm, gate_v), (up_hbm, up_v), (down_hbm, down_v)):
-            mate_kept.append(remote(src.at[plane], dst.at[j], me_e, t))
+        for kind, (src, dst) in enumerate(
+            ((gate_hbm, gate_v), (up_hbm, up_v), (down_hbm, down_v))
+        ):
+            mate_kept.append(remote(src.at[plane], dst.at[j], me_e, t, ("kept", kind, j)))
 
     group_size = HEADS // KV_HEADS
     blocks = q_v.shape[0] // WINDOW
@@ -379,23 +415,29 @@
         projected = jnp.dot(mix[rows, :], out_w[...], preferred_element_type=F32)
         mixer_ref[rows, :] = rms_scale(projected, att_gain_ref[...]).astype(BF16)
 
-    def relay(copy, view):
+    def relay(copy, view, kind):
         copy.wait_recv()
-        return [remote(view(far), view(far + j), me_e, t) for j, t in enumerate(mates, 1)]
+        return [
+            remote(view(far), view(far + j), me_e, t, ("relay", kind, j))
+            for j, t in enumerate(mates, 1)
+        ]
 
     for load in load_q[:3]:
         load.wait()
     for n in range(1, blocks):
         attend(n)
-    gate_mate = relay(gate_far[0], lambda b: gate_v.at[b, first_rows])
-    for copy in rims:
-        copy.wait_recv()
-    before_at = (before // n_tp, lax.rem(before, n_tp))
-    pl.semaphore_signal(ack_sem, inc=1, device_id=before_at, device_id_type=MESH)
-    attend(0)
+    gate_mate = relay(gate_far[0], lambda b: gate_v.at[b, first_rows], 0)
     load_q[3].wait()
-    for n in range(blocks):
+    for n in range(1, blocks):
         project(n)
+
+    def attend_rim():
+        for copy in rims:
+            copy.wait_recv()
+        before_at = (before // n_tp, lax.rem(before, n_tp))
+        pl.semaphore_signal(ack_sem, inc=1, device_id=before_at, device_id_type=MESH)
+        attend(0)
+        project(0)
 
     def share(side, rows_ref):
         rows = rows_ref[...]
@@ -430,29 +472,34 @@
         def _():
             empty = pl.ds(pl.multiple_of((1 - upper) * (slots // 2), slots // 2), slots // 2)
             for side in range(2):
-                for c in range(CHUNKS):
-                    returned[side, c, empty, :] = jnp.zeros((slots // 2, cw), BF16)
+                returned[side, empty, :] = jnp.zeros((slots // 2, d), BF16)
 
     def product(side, weights, low, count):
         rows = arrived[side]
         matrix = weights[low : low + count].reshape(count * width, d)
         return lax.dot_general(rows, matrix, NT, preferred_element_type=F32)
 
-    gate_mate += relay(gate_far[1], lambda b: gate_v.at[b, last_rows])
+    gate_mate += relay(gate_far[1], lambda b: gate_v.at[b, last_rows], 0)
     for load in own_loads:
         load.wait()
     for copy in mate_kept:
         copy.wait_recv()
     for copy in gate_mate:
         copy.wait_recv()
-    wait_rows(0, packed.at[0], arrived.at[0])
+    wait_dispatch(0)
     act[0] = silu(product(0, gate_v, 0, 2 * far))
     hidden[0, :, :half] = (act[0, :, :half] * product(0, up_v, 0, far)).astype(BF16)
-    up_mate = relay(up_far[0], lambda b: up_v.at[b, up_halves[0]])
-    wait_rows(1, packed.at[1], arrived.at[1])
+    up_mate = relay(up_far[0], lambda b: up_v.at[b, up_halves[0]], 1)
+    up_mate += relay(up_far[1], lambda b: up_v.at[b, up_halves[1]], 1)
+    wait_dispatch(1)
     act[1] = silu(product(1, gate_v, 0, 2 * far))
     hidden[1, :, :half] = (act[1, :, :half] * product(1, up_v, 0, far)).astype(BF16)
-    up_mate += relay(up_far[1], lambda b: up_v.at[b, up_halves[1]])
+
+    def relay_down(c):
+        cols = chunks[c]
+        return relay(down_far[c], lambda b: down_v.at[b, :, cols], 2)
+
+    down_mate = relay_down(0)
     for copy in up_mate:
         copy.wait_recv()
     for side in range(2):
@@ -484,10 +531,10 @@
         )
         return [
             pltpu.make_async_remote_copy(
-                outs.at[side, c, rows_of(home)],
-                home_rows.at[c, pl.ds(n * cap, cap)],
-                home_send.at[c, n],
-                home_recv.at[c, n],
+                outs.at[side, rows_of(home), chunks[c]],
+                home_rows.at[pl.ds(n * cap, cap), chunks[c]],
+                home_send.at[1],
+                home_recv.at[c, 1],
                 device_id=(e, t),
                 device_id_type=MESH,
             )
@@ -497,9 +544,9 @@
     def home_step(c):
         to = end_flag * (1 + line // last) + (1 - end_flag) * home_line
         return pltpu.make_async_remote_copy(
-            home_out.at[c],
-            home_in.at[c],
-            home_send.at[c, 0],
+            home_out.at[:, chunks[c]],
+            home_in.at[:, chunks[c]],
+            home_send.at[0],
             home_recv.at[c, 0],
             device_id=(to * PAIR + spot, me_t),
             device_id_type=MESH,
@@ -508,27 +555,35 @@
     def gather_home(c):
         for copy in home_blocks(c):
             copy.start()
-        home_rows[c, 0:cap, :] = outs[0, c, rows_of(home_line * PAIR + spot), :]
+        home_rows[0:cap, chunks[c]] = outs[0, rows_of(home_line * PAIR + spot), chunks[c]]
 
     def sum_home(c):
-        for copy in home_blocks(c):
-            copy.wait_recv()
-        sums = weigh(None, home_columns, home_chosen[...], home_rows[c])
+        view = home_rows.at[pl.ds(0, (2 * PAIR - 1) * cap), chunks[c]]
+        pltpu.make_async_remote_copy(
+            view,
+            view,
+            home_send.at[1],
+            home_recv.at[c, 1],
+            device_id=(me_e, away),
+            device_id_type=MESH,
+        ).wait_recv()
+        sums = weigh(None, home_columns, home_chosen[...], home_rows[:, chunks[c]])
 
         @pl.when(at_end)
         def _():
-            home_out[c] = sums.astype(BF16)
+            home_out[:, chunks[c]] = sums.astype(BF16)
             home_step(c).start()
 
         @pl.when(jnp.logical_not(at_end))
         def _():
-            home_sums[c] = sums
+            home_sums[:, chunks[c]] = sums
 
     def pass_home(c):
         @pl.when(jnp.logical_not(at_end))
         def _():
             home_step(c).wait_recv()
-            home_out[c] = (home_sums[c] + home_in[c].astype(F32)).astype(BF16)
+            sums = home_sums[:, chunks[c]] + home_in[:, chunks[c]].astype(F32)
+            home_out[:, chunks[c]] = sums.astype(BF16)
             home_step(c).start()
 
     if merging:
@@ -537,24 +592,29 @@
     def send_back(side, c, first):
         exchange(
             phase(side, c),
-            outs.at[side, c],
-            returned.at[side, c],
-            lambda copy: copy.start(),
+            outs.at[side],
+            returned.at[side],
+            chunks[c],
             is_sent if merging else None,
             first,
             2,
         )
 
     for c, cols in enumerate(chunks):
-        for copy in relay(down_far[c], lambda b, cols=cols: down_v.at[b, :, cols]):
+        if c:
+            down_mate = relay_down(c)
+        for copy in down_mate:
             copy.wait_recv()
-        matrix = down_v[:, :, cols].reshape(2 * half, cw)
+        matrix = down_v[:, :, cols].reshape(2 * half, WIDTHS[c] * unit)
         for side in range(2):
-            outs[side, c] = jnp.dot(hidden[side], matrix, preferred_element_type=F32).astype(BF16)
+            outs[side, :, cols] = jnp.dot(hidden[side], matrix, preferred_element_type=F32).astype(BF16)
         if merging:
             gather_home(c)
         if c + AHEAD < CHUNKS:
             down_far[c + AHEAD].start()
+        if c + AHEAD == CHUNKS:
+            for copy in rims:
+                copy.start()
         if merging:
             if c:
                 sum_home(c - 1)
@@ -564,7 +624,7 @@
             send_back(side, c, 2)
             if c < EARLY:
                 send_back(side, c, 1)
-            keep_rows(outs.at[side, c], returned.at[side, c])
+            keep_rows(outs.at[side], returned.at[side], cols)
         if merging and c >= 2:
             pass_home(c - 2)
     for c in range(EARLY, CHUNKS):
@@ -573,53 +633,63 @@
 
     scales = [columns_of(weight_ref[...]), columns_of(far_weight[...])]
 
+    def wait_back(side, c):
+        if not merging:
+            wait_rows(phase(side, c), returned.at[side], chunks[c], n_ep - 1)
+            return
+
+        @pl.when(at_end)
+        def _():
+            wait_rows(phase(side, c), returned.at[side], chunks[c], n_ep // 2 - 1)
+
+        @pl.when(jnp.logical_not(at_end))
+        def _():
+            wait_rows(phase(side, c), returned.at[side], chunks[c], n_ep - 1)
+
     def combine(side, c):
-        wait_rows(phase(side, c), outs.at[side, c], returned.at[side, c], True)
-        return weigh(shared[side, :, chunks[c]], scales[side], chosen[side], returned[side, c])
+        wait_back(side, c)
+        cols = chunks[c]
+        return weigh(shared[side, :, cols], scales[side], chosen[side], returned[side, :, cols])
 
     parts = []
     for c, cols in enumerate(chunks):
-        if merging and c % 2 == 0:
-            pass_home(CHUNKS - 2 + c // 2)
-        for side in (1, 0):
-            if side:
-                part_out[c] = combine(1, c).astype(BF16)
-                parts.append(remote(part_out.at[c], part_in.at[c], me_e, away))
-            else:
-                shared[0, :, cols] = combine(0, c)
+        if merging and c == 0:
+            pass_home(CHUNKS - 2)
+        if merging and c == EARLY:
+            pass_home(CHUNKS - 1)
+        if c == EARLY:
+            attend_rim()
+        part_out[:, cols] = combine(1, c).astype(BF16)
+        parts.append(remote(part_out.at[:, cols], part_in.at[:, cols], me_e, away, "part"))
+        shared[0, :, cols] = combine(0, c)
+
+    wait_sent(0, packed, n_ep - 1)
+    wait_sent(1, outs, n_ep - 1 - (PAIR if merging else 0))
+    settle("ids", ids_ref)
+    settle("weight", weight_ref)
+    settle("normed", normed)
+    settle("rim_k", rim_k)
+    settle("rim_v", rim_v)
+    for name, ref in (("gate", gate_hbm), ("up", up_hbm), ("down", down_hbm)):
+        settle(name, ref.at[other])
+    for j in range(1, far):
+        for kind, ref in enumerate((gate_v, up_v, down_v)):
+            settle(("kept", kind, j), ref.at[0])
+            settle(("relay", kind, j), ref.at[far])
+        for kind, ref in enumerate((common_gate_hbm, common_up_hbm, common_down_hbm)):
+            settle(("common", kind, j), ref)
     if merging:
-
-        @pl.when(at_end)
-        def _():
-            for c, cols in enumerate(chunks):
-                home_step(c).wait_recv()
-                shared[0, :, cols] += home_in[c].astype(F32)
-
-    square = jnp.zeros((tokens, 1), F32)
-    for c, cols in enumerate(chunks):
-        parts[c].wait_recv()
-        total = shared[0, :, cols] + part_in[c].astype(F32)
-        shared[0, :, cols] = total
-        square = square + jnp.sum(total * total, axis=-1, keepdims=True)
-    scale = lax.rsqrt(square * (1.0 / d) + EPS)
-    experts_ref[...] = (shared[0] * scale * moe_gain_ref[...]).astype(BF16)
-
-    for copy in sent:
-        copy.wait_send()
-    for side in range(2):
-        exchange(side, packed.at[side], arrived.at[side], lambda copy: copy.wait_send())
-        for c in range(CHUNKS):
-            exchange(
-                phase(side, c),
-                outs.at[side, c],
-                returned.at[side, c],
-                lambda copy: copy.wait_send(),
-                is_sent if merging else None,
-            )
+        for n, view in enumerate((home_out, home_rows.at[pl.ds(0, (2 * PAIR - 1) * cap)])):
+            pltpu.make_async_remote_copy(
+                view,
+                view,
+                home_send.at[n],
+                home_recv.at[0, 0],
+                device_id=(me_e, away),
+                device_id_type=MESH,
+            ).wait_send()
+    pl.semaphore_wait(ack_sem, 1)
     if merging:
-        for c in range(CHUNKS):
-            for copy in home_blocks(c) + [home_step(c)]:
-                copy.wait_send()
 
         @pl.when(at_end)
         def _():
@@ -627,7 +697,23 @@
                 for copy in home_meta(n):
                     copy.wait_send()
 
-    pl.semaphore_wait(ack_sem, 1)
+    square = jnp.zeros((tokens, 1), F32)
+    for c, cols in enumerate(chunks):
+        if merging:
+
+            @pl.when(at_end)
+            def _():
+                home_step(c).wait_recv()
+                shared[0, :, cols] += home_in[:, cols].astype(F32)
+
+        parts[c].wait_recv()
+        total = shared[0, :, cols] + part_in[:, cols].astype(F32)
+        shared[0, :, cols] = total
+        square = square + jnp.sum(total * total, axis=-1, keepdims=True)
+    scale = lax.rsqrt(square * (1.0 / d) + EPS)
+    experts_ref[...] = (shared[0] * scale * moe_gain_ref[...]).astype(BF16)
+    settle("part", part_out)
+    assert not sent
 
 
 def body(
@@ -662,7 +748,6 @@
     kv = att_keys.shape[1]
     units = w_gate.shape[2]
     common = common_expert_gate_weight.shape[1]
-    cw = d // CHUNKS
     scratch = [
         pltpu.VMEM((tokens, d), BF16),
         pltpu.VMEM((tokens, d), BF16),
@@ -672,8 +757,8 @@
         pltpu.VMEM((2, slots, top * tokens), BF16),
         pltpu.VMEM((2, slots, d), BF16),
         pltpu.VMEM((2, slots, d), BF16),
-        pltpu.VMEM((2, CHUNKS, slots, cw), BF16),
-        pltpu.VMEM((2, CHUNKS, slots, cw), BF16),
+        pltpu.VMEM((2, slots, d), BF16),
+        pltpu.VMEM((2, slots, d), BF16),
         pltpu.VMEM((blocks, units, d), BF16),
         pltpu.VMEM((blocks, units, d), BF16),
         pltpu.VMEM((blocks, units, d), BF16),
@@ -683,8 +768,8 @@
         pltpu.VMEM((d, far * common), BF16),
         pltpu.VMEM((far * common, d), BF16),
         pltpu.VMEM((2, tokens, d), F32),
-        pltpu.VMEM((CHUNKS, tokens, cw), BF16),
-        pltpu.VMEM((CHUNKS, tokens, cw), BF16),
+        pltpu.VMEM((tokens, d), BF16),
+        pltpu.VMEM((tokens, d), BF16),
         pltpu.VMEM((rows, width), BF16),
         pltpu.VMEM((rows, kv), BF16),
         pltpu.VMEM((rows, kv), BF16),
@@ -693,10 +778,10 @@
         pltpu.VMEM(out_weight.shape, BF16),
         pltpu.VMEM((rows, width), BF16),
         pltpu.SemaphoreType.DMA((11,)),
+        pltpu.SemaphoreType.DMA((9 + (far - 1) * 9,)),
         pltpu.SemaphoreType.DMA((9 + 2 * CHUNKS + (far - 1) * (10 + CHUNKS),)),
-        pltpu.SemaphoreType.DMA((9 + 2 * CHUNKS + (far - 1) * (10 + CHUNKS),)),
-        pltpu.SemaphoreType.DMA((2 + 2 * CHUNKS, n_ep)),
-        pltpu.SemaphoreType.DMA((2 + 2 * CHUNKS, n_ep)),
+        pltpu.SemaphoreType.DMA((2,)),
+        pltpu.SemaphoreType.DMA((2 + 2 * CHUNKS,)),
         pltpu.SemaphoreType.REGULAR,
     ]
     if n_ep == PAIR * LINE and far == 2:
@@ -704,14 +789,14 @@
             pltpu.VMEM((top, tokens), jnp.int32),
             pltpu.VMEM((top, tokens), F32),
             pltpu.VMEM((2 * PAIR * cap, top * tokens), BF16),
-            pltpu.VMEM((CHUNKS, 2 * PAIR * cap, cw), BF16),
-            pltpu.VMEM((CHUNKS, tokens, cw), F32),
-            pltpu.VMEM((CHUNKS, tokens, cw), BF16),
-            pltpu.VMEM((CHUNKS, tokens, cw), BF16),
+            pltpu.VMEM((2 * PAIR * cap, d), BF16),
+            pltpu.VMEM((tokens, d), F32),
+            pltpu.VMEM((tokens, d), BF16),
+            pltpu.VMEM((tokens, d), BF16),
             pltpu.SemaphoreType.DMA((2, 2)),
             pltpu.SemaphoreType.DMA((2,)),
-            pltpu.SemaphoreType.DMA((CHUNKS, 4)),
-            pltpu.SemaphoreType.DMA((CHUNKS, 4)),
+            pltpu.SemaphoreType.DMA((2,)),
+            pltpu.SemaphoreType.DMA((CHUNKS, 2)),
         ]
     return pl.pallas_call(
         functools.partial(layer_kernel, n_ep, n_tp, cap),

time: 106 us -> 103 us (0.972)
  Pallas kernels: 104 us -> 100 us
    pallas_call x1, Pallas kernels: 104 us -> 100 us  [body(): pl.pallas_call(functools.partial(layer_kernel, n_ep, n_tp, cap), out_shap...]
where the time goes in v2:
time: 103 us; the launch traced here: 102 us
  Pallas kernels  100 us (97%)
  local copies, waits for them, and re-layouts  1.77 us (2%)
    pallas_call x1, Pallas kernels, body(): pl.pallas_call(functools.partial(layer_kernel, n_ep, n_tp, cap), out_shap...  100 us

profile of v2, /device:TPU:0, one launch (start us, length us, event | category | flops | bytes accessed | tf_op | source)
XLA Modules:
  0.0 102.4 jit_solution(4858300114518745228)
XLA Ops:
  0.6 100.0 %layer.1 = (bf16[256,2048]{1,0:T(8,128)(2,1)S(1)}, bf16[128,2048]{1,0:T(8,128)(2,1)S(1)}) custom-call(f32[16]{0:T(128)} %sink_ref.1, s32[2,128]{1,0:T(2,128)} %bitcast.12, f32[2,128]{1,0:T(2,128)} %bitcast.13, f32[1,2048]{1,0:T(1,128)} %bitcast.9, f32[1,2048]{1,0:T(1,128)} %bitcast.10, f32[1,2048]{1,0:T(1,128)} %bitcast.11, bf16[256,1024]{1,0:T(8,128)(2,1)} %q_hbm.1, ...), custom_call_target="tpu_custom_call" | custom-call | tf_op jit(solution)/shard_map/layer/pallas_call | solution.py:801
  100.6 1.0 copy.21
  101.6 0.8 copy.22

commit v3 on v2

--- a/solution.py
+++ b/solution.py
@@ -268,6 +268,35 @@
         fetch(common_up_hbm, common_up.at[:, pl.ds(0, common_cols)]),
         fetch(common_down_hbm, common_down.at[pl.ds(0, common_cols)]),
     ]
+    load_x.wait()
+    normed[...] = rms_scale(x_v[...].astype(F32), pre_gain_ref[...]).astype(BF16)
+    earlier = (iota((tokens, tokens), 0) < iota((tokens, tokens), 1)).astype(F32).astype(BF16)
+
+    def route(ids, numbers, chosen_ref):
+        hits = [numbers == ids[k : k + 1, :] for k in range(top)]
+        hit = functools.reduce(lambda a, b: a | b, hits).astype(F32).astype(BF16)
+        count = jnp.dot(hit, earlier, preferred_element_type=F32)
+        place = count + (iota(numbers.shape, 0) * cap + 1).astype(F32)
+        slot_number = (iota((chosen_ref.shape[0], tokens), 0) + 1).astype(F32)
+        total = None
+        for k in range(top):
+            slot = jnp.sum(jnp.where(hits[k], place, 0.0), axis=0, keepdims=True)
+            one_hot = (slot_number == slot).astype(F32).astype(BF16)
+            chosen_ref[:, k * tokens : (k + 1) * tokens] = one_hot
+            total = one_hot if total is None else total + one_hot
+        return total
+
+    def pack(ids, side, rows_ref):
+        numbers = iota((n_ep, tokens), 0) * PLANES + plane
+        one_hot = route(ids, numbers, chosen.at[side])
+        rows = rows_ref[...]
+        step = slots // 2
+        for i in range(2):
+            packed[side, i * step : (i + 1) * step, :] = jnp.dot(
+                one_hot[i * step : (i + 1) * step], rows, preferred_element_type=F32
+            ).astype(BF16)
+
+    pack(ids_ref[...], 0, normed)
     pl.semaphore_wait(barrier, n_ep - 1 + far + 2 + int(merging))
 
     cut = width // 4
@@ -321,8 +350,6 @@
                 for copy in home_meta(n):
                     copy.start()
 
-    load_x.wait()
-    normed[...] = rms_scale(x_v[...].astype(F32), pre_gain_ref[...]).astype(BF16)
     normed_far = remote(normed, far_normed, me_e, away, "normed")
     gate_far.append(
         remote(gate_hbm.at[other, last_rows], gate_v.at[far, last_rows], me_e, away, "gate")
@@ -339,35 +366,11 @@
         for c, cols in enumerate(chunks)
     ]
 
-    earlier = (iota((tokens, tokens), 0) < iota((tokens, tokens), 1)).astype(F32).astype(BF16)
-
-    def route(ids, numbers, chosen_ref):
-        hits = [numbers == ids[k : k + 1, :] for k in range(top)]
-        hit = functools.reduce(lambda a, b: a | b, hits).astype(F32).astype(BF16)
-        count = jnp.dot(hit, earlier, preferred_element_type=F32)
-        place = count + (iota(numbers.shape, 0) * cap + 1).astype(F32)
-        slot_number = (iota((chosen_ref.shape[0], tokens), 0) + 1).astype(F32)
-        total = None
-        for k in range(top):
-            slot = jnp.sum(jnp.where(hits[k], place, 0.0), axis=0, keepdims=True)
-            one_hot = (slot_number == slot).astype(F32).astype(BF16)
-            chosen_ref[:, k * tokens : (k + 1) * tokens] = one_hot
-            total = one_hot if total is None else total + one_hot
-        return total
-
-    def pack(ids, side, rows_ref):
-        numbers = iota((n_ep, tokens), 0) * PLANES + plane
-        one_hot = route(ids, numbers, chosen.at[side])
-        rows = rows_ref[...]
-        step = slots // 2
-        for i in range(2):
-            packed[side, i * step : (i + 1) * step, :] = jnp.dot(
-                one_hot[i * step : (i + 1) * step], rows, preferred_element_type=F32
-            ).astype(BF16)
+    def dispatch(side):
         exchange(side, packed.at[side], arrived.at[side], everything)
         keep_rows(packed.at[side], arrived.at[side], everything)
 
-    pack(ids_ref[...], 0, normed)
+    dispatch(0)
     for j, t in enumerate(mates, 1):
         for kind, (src, dst) in enumerate(
             ((gate_hbm, gate_v), (up_hbm, up_v), (down_hbm, down_v))
@@ -456,6 +459,7 @@
         copy.wait_recv()
     normed_far.wait_recv()
     pack(far_ids[...], 1, far_normed)
+    dispatch(1)
     share(1, far_normed)
 
     if merging:
@@ -621,15 +625,15 @@
             if c == CHUNKS - 1:
                 sum_home(c)
         for side in (1, 0):
-            send_back(side, c, 2)
+            if side or c <= EARLY:
+                send_back(side, c, 2)
             if c < EARLY:
                 send_back(side, c, 1)
             keep_rows(outs.at[side], returned.at[side], cols)
         if merging and c >= 2:
             pass_home(c - 2)
     for c in range(EARLY, CHUNKS):
-        for side in (1, 0):
-            send_back(side, c, 1)
+        send_back(1, c, 1)
 
     scales = [columns_of(weight_ref[...]), columns_of(far_weight[...])]
 
@@ -652,16 +656,32 @@
         return weigh(shared[side, :, cols], scales[side], chosen[side], returned[side, :, cols])
 
     parts = []
-    for c, cols in enumerate(chunks):
-        if merging and c == 0:
-            pass_home(CHUNKS - 2)
-        if merging and c == EARLY:
-            pass_home(CHUNKS - 1)
-        if c == EARLY:
-            attend_rim()
+
+    def combine_far(c):
+        cols = chunks[c]
         part_out[:, cols] = combine(1, c).astype(BF16)
         parts.append(remote(part_out.at[:, cols], part_in.at[:, cols], me_e, away, "part"))
-        shared[0, :, cols] = combine(0, c)
+
+    def combine_own(c):
+        shared[0, :, chunks[c]] = combine(0, c)
+
+    for c in range(EARLY):
+        combine_far(c)
+    if merging:
+        pass_home(CHUNKS - 2)
+    for c in range(EARLY):
+        combine_own(c)
+    if merging:
+        pass_home(CHUNKS - 1)
+    for c in range(EARLY, CHUNKS):
+        if c > EARLY:
+            send_back(0, c, 2)
+        send_back(0, c, 1)
+    attend_rim()
+    for c in range(EARLY, CHUNKS):
+        combine_far(c)
+    for c in range(EARLY, CHUNKS):
+        combine_own(c)
 
     wait_sent(0, packed, n_ep - 1)
     wait_sent(1, outs, n_ep - 1 - (PAIR if merging else 0))

time: 103 us -> 101 us (0.981)
  Pallas kernels: 100 us -> 98.1 us
    pallas_call x1, Pallas kernels: 100 us -> 98.1 us  [body(): pl.pallas_call(functools.partial(layer_kernel, n_ep, n_tp, cap), out_shap...]
where the time goes in v3:
time: 101 us; the launch traced here: 100 us
  Pallas kernels  98.1 us (97%)
  local copies, waits for them, and re-layouts  1.77 us (2%)
    pallas_call x1, Pallas kernels, body(): pl.pallas_call(functools.partial(layer_kernel, n_ep, n_tp, cap), out_shap...  98.1 us

profile of v3, /device:TPU:0, one launch (start us, length us, event | category | flops | bytes accessed | tf_op | source)
XLA Modules:
  0.0 100.5 jit_solution(14934186301938526129)
XLA Ops:
  0.6 98.1 %layer.1 = (bf16[256,2048]{1,0:T(8,128)(2,1)S(1)}, bf16[128,2048]{1,0:T(8,128)(2,1)S(1)}) custom-call(f32[16]{0:T(128)} %sink_ref.1, s32[2,128]{1,0:T(2,128)} %bitcast.12, f32[2,128]{1,0:T(2,128)} %bitcast.13, f32[1,2048]{1,0:T(1,128)} %bitcast.9, f32[1,2048]{1,0:T(1,128)} %bitcast.10, f32[1,2048]{1,0:T(1,128)} %bitcast.11, bf16[256,1024]{1,0:T(8,128)(2,1)} %q_hbm.1, ...), custom_call_target="tpu_custom_call" | custom-call | tf_op jit(solution)/shard_map/layer/pallas_call | solution.py:821
  98.7 1.0 copy.21
  99.7 0.8 copy.22
